TPU v7x, 32 devices: a whole 2x2x4 slice. The times are simulated.
32 devices in a mesh: fs: 16 (over z, y, x), tp: 2 (over core).
Axes of the slice: x: 2, y: 2, z: 4, core: 2. Of those that a mesh axis runs over, the one named last changes fastest.
Arguments:
- inputs: bfloat16 [8192, 2048], P('fs', 'tp'), may hold values from -6 to 6
- value_cotangent: bfloat16 [8192, 2048], P('fs', 'tp'), may hold values from -6 to 6
- first_map: bfloat16 [8192, 2048], P('fs', 'tp'), may hold values from -6 to 6
- second_map: bfloat16 [8192, 2048], P('fs', 'tp'), may hold values from -6 to 6
- lambdas: float32 [16], P('tp'), may hold values from 0.3 to 0.8
- head_gain: float32 [128], replicated, may hold values from 0.1 to 1.9
- output_cotangent: bfloat16 [8192, 2048], P('fs', 'tp'), may hold values from -6 to 6
- value_factor: bfloat16 [2048, 256], replicated, may hold values from -0.125 to 0.125
- output_factor: bfloat16 [2048, 256], replicated, may hold values from -0.125 to 0.125
- value_weight: float32 [2048, 2048], P('fs', 'tp'), may hold values from -0.125 to 0.125
- output_weight: float32 [2048, 2048], P('tp', 'fs'), may hold values from -0.125 to 0.125
- value_moment: float32 [256, 2048], P('fs', 'tp'), may hold values from -6 to 6
- value_second: float32 [256, 2048], P('fs', 'tp'), may hold values from 0.25 to 4
- output_moment: float32 [256, 2048], P('fs', 'tp'), may hold values from -6 to 6
- output_second: float32 [256, 2048], P('fs', 'tp'), may hold values from 0.25 to 4
Outputs:
- value_master: float32 [2048, 2048], P('fs', 'tp')
- output_master: float32 [2048, 2048], P('tp', 'fs')
- value_moment_new: float32 [256, 2048], P('fs', 'tp')
- value_second_new: float32 [256, 2048], P('fs', 'tp')
- output_moment_new: float32 [256, 2048], P('fs', 'tp')
- output_second_new: float32 [256, 2048], P('fs', 'tp')
- value_copy: bfloat16 [2048, 2048], P(None, 'tp')
- output_copy: bfloat16 [2048, 2048], P('tp')
All inputs are finite; a program needn't handle non-finite values.
Results may differ from a plain program's by a relative error of at most 0.0027.
Values may be sent and summed in bfloat16 or wider, within the bound.
A program may use at most 64 MiB of HBM per device.

v0:
```python
import math
import jax
import jax.numpy as jnp
from jax import lax
from jax.sharding import PartitionSpec as P


def contract_rows(left, right, precise):
    if precise:
        return lax.dot_general(
            left,
            right,
            (((0,), (0,)), ((), ())),
            precision=lax.Precision.HIGHEST,
            preferred_element_type=jnp.float32,
        )
    return lax.dot_general(
        left, right, (((0,), (0,)), ((), ())), preferred_element_type=jnp.float32
    )


def local(
    inputs,
    value_cotangent,
    first_map,
    second_map,
    lambdas,
    head_gain,
    output_cotangent,
    value_factor,
    output_factor,
    value_weight,
    output_weight,
    value_moment,
    value_second,
    output_moment,
    output_second,
):
    tok_rows = inputs.shape[0]
    local_heads = lambdas.shape[0]
    head_width = head_gain.shape[0]
    head_cols = local_heads * head_width
    first = first_map.astype(jnp.float32).reshape(tok_rows, local_heads, head_width)
    second = second_map.astype(jnp.float32).reshape(tok_rows, local_heads, head_width)
    difference = first - lambdas[None, :, None] * second
    normed = (
        difference
        * lax.rsqrt(jnp.mean(difference * difference, axis=-1, keepdims=True) + 1e-06)
        * head_gain
    )
    heads_out = normed.reshape(tok_rows, head_cols).astype(jnp.bfloat16)
    full_inputs, full_cotangent = (
        lax.all_gather(inputs, "tp", axis=1, tiled=True),
        lax.all_gather(output_cotangent, "tp", axis=1, tiled=True),
    )
    token_scale = 1.0 / math.sqrt(tok_rows * lax.axis_size("fs"))
    fs_index = lax.axis_index("fs")
    width_rows = value_weight.shape[0]
    value_rows = lax.dynamic_slice_in_dim(
        value_factor, fs_index * width_rows, width_rows, 0
    ).astype(jnp.float32)
    output_rows = lax.dynamic_slice_in_dim(
        output_factor, fs_index * width_rows, width_rows, 0
    ).astype(jnp.float32)
    grad_value = contract_rows(full_inputs, value_cotangent, False) * token_scale
    grad_output = contract_rows(full_cotangent, heads_out, False) * token_scale
    partial_value = jnp.concatenate(
        [
            contract_rows(value_factor.astype(jnp.float32), grad_value, True),
            contract_rows(output_factor.astype(jnp.float32), grad_output, True),
        ],
        axis=1,
    )
    own_rows = lax.psum_scatter(partial_value, "fs", scatter_dimension=0, tiled=True)
    moments = jnp.concatenate([value_moment, output_moment], axis=1)
    seconds = jnp.concatenate([value_second, output_second], axis=1)
    moment_new = 0.8 * moments + 0.2 * own_rows
    second_new = 0.95 * seconds + 0.05 * own_rows * own_rows
    direction = moment_new / (jnp.sqrt(second_new) + 1e-08)
    full_direction = lax.all_gather(direction, "fs", axis=0, tiled=True)
    step_value = jnp.dot(
        value_rows,
        full_direction[:, :head_cols],
        precision=lax.Precision.HIGHEST,
        preferred_element_type=jnp.float32,
    )
    step_output = jnp.dot(
        output_rows,
        full_direction[:, head_cols:],
        precision=lax.Precision.HIGHEST,
        preferred_element_type=jnp.float32,
    )
    value_master = value_weight - 0.05 * step_value
    output_master = output_weight - 0.05 * step_output.T
    value_copy, output_copy = (
        lax.all_gather(value_master.astype(jnp.bfloat16), "fs", axis=0, tiled=True),
        lax.all_gather(output_master.astype(jnp.bfloat16), "fs", axis=1, tiled=True),
    )
    return (
        value_master,
        output_master,
        moment_new[:, :head_cols],
        second_new[:, :head_cols],
        moment_new[:, head_cols:],
        second_new[:, head_cols:],
        value_copy,
        output_copy,
    )


def solution(mesh):
    in_specs = (
        P("fs", "tp"),
        P("fs", "tp"),
        P("fs", "tp"),
        P("fs", "tp"),
        P("tp"),
        P(),
        P("fs", "tp"),
        P(),
        P(),
        P("fs", "tp"),
        P("tp", "fs"),
        P("fs", "tp"),
        P("fs", "tp"),
        P("fs", "tp"),
        P("fs", "tp"),
    )
    out_specs = (
        P("fs", "tp"),
        P("tp", "fs"),
        P("fs", "tp"),
        P("fs", "tp"),
        P("fs", "tp"),
        P("fs", "tp"),
        P(None, "tp"),
        P("tp", None),
    )
    return jax.shard_map(local, mesh=mesh, in_specs=in_specs, out_specs=out_specs, check_vma=False)
```

profile of v0, /device:TPU:0, one launch (start us, length us, event | category | flops | bytes accessed | tf_op | source)
XLA Modules:
  0.0 374.0 jit_solution(844891537116236253)
XLA Ops:
  7.2 0.0 copy-start
  7.2 0.0 all-gather.8.cloned.1.call-start
  7.2 0.7 all-gather.8.cloned.1.call-update
  7.9 0.0 all-gather.6.cloned.1.call-start
  8.0 0.7 all-gather.6.cloned.1.call-update
  8.7 0.0 reduce-scatter.4.cloned.1.call-start
  8.7 0.2 convert_bitcast_fusion
  9.0 0.0 copy-start.2
  9.0 0.5 copy.52
  9.5 0.7 copy-done.2
  10.2 0.2 convert_bitcast_fusion.1
  10.5 0.5 copy.51
  11.0 0.2 copy-done.15
  11.1 0.3 fusion.9
  11.4 0.0 copy-start.16
  11.4 0.6 multiply_reduce_fusion
  12.0 0.1 copy.44
  12.2 0.1 copy.45
  12.3 0.1 broadcast_bitcast_fusion
  12.4 10.5 %all-gather.8.cloned.1.call-done = bf16[512,2048]{1,0:T(8,128)(2,1)} async-done(((bf16[512,1024]{1,0:T(8,128)(2,1)}), bf16[512,2048]{1,0:T(8,128)(2,1)}) %all-gather.8.cloned.1.call-update) | async-done | bytes 2097168 | tf_op jit(solution)/shard_map/all_gather | solution.py:54
  22.9 0.6 mul.105
  23.5 1.0 copy-done.5
  24.5 2.8 fusion.18
  27.3 4.0 %fusion.13 = f32[256,1024]{0,1:T(8,128)S(1)} fusion(bf16[2048,256]{1,0:T(8,128)(2,1)S(1)} %copy-done.8, f32[1024,2048]{1,0:T(8,128)S(1)} %fusion.18), kind=kOutput, calls=%fused_computation.18 | convolution fusion | flops 6444548096 | bytes 10485760 | tf_op jit(solution)/shard_map/dot_general | solution.py:10
  31.4 4.8 %all-gather.6.cloned.1.call-done = bf16[512,2048]{1,0:T(8,128)(2,1)} async-done(((bf16[512,1024]{1,0:T(8,128)(2,1)}), bf16[512,2048]{1,0:T(8,128)(2,1)}) %all-gather.6.cloned.1.call-update) | async-done | bytes 2097168 | tf_op jit(solution)/shard_map/all_gather | solution.py:53
  36.2 4.0 %fusion.38 = f32[2048,1024]{1,0:T(8,128)S(1)} fusion(bf16[512,2048]{1,0:T(8,128)(2,1)} %all-gather.6.cloned.1.call-done, bf16[512,1024]{1,0:T(8,128)(2,1)S(1)} %copy-done), kind=kOutput, calls=%fused_computation.47 | convolution fusion | flops 2147483648 | bytes 11534336 | tf_op jit(solution)/shard_map/dot_general | solution.py:17
  40.2 6.9 %fusion.10 = f32[256,1024]{0,1:T(8,128)S(1)} fusion(bf16[2048,256]{1,0:T(8,128)(2,1)S(1)} %copy-done.7, f32[2048,1024]{1,0:T(8,128)S(1)} %fusion.38), kind=kOutput, calls=%fused_computation.17 | convolution fusion | flops 6444548096 | bytes 10485760 | tf_op jit(solution)/shard_map/dot_general | solution.py:10
  47.2 0.1 pad_maximum_fusion
  47.3 1.8 copy.49
  49.2 0.0 reduce-scatter.4.cloned.1.call-update
  49.2 0.0 copy-start.10
  49.2 0.0 all-gather.10.cloned.1.call-start
  49.3 82.7 %reduce-scatter.4.cloned.1.call-done = f32[16,2048]{1,0:T(8,128)} async-done(((f32[256,2048]{1,0:T(8,128)}), f32[16,2048]{1,0:T(8,128)}) %reduce-scatter.4.cloned.1.call-update) | async-done | bytes 131088 | tf_op jit(solution)/shard_map/reduce_scatter | solution.py:74
  132.0 1.6 add_divide_fusion
  133.7 0.0 all-gather.10.cloned.1.call-update
  133.7 0.0 all-gather.12.cloned.1.call-start
  133.7 58.5 %all-gather.10.cloned.1.call-done = f32[256,2048]{1,0:T(8,128)} async-done(((f32[16,2048]{1,0:T(8,128)}), f32[256,2048]{1,0:T(8,128)}) %all-gather.10.cloned.1.call-update) | async-done | bytes 2097168 | tf_op jit(solution)/shard_map/all_gather | solution.py:80
  192.2 2.8 fusion.36
  195.0 0.0 all-gather.12.cloned.1.call-update
  195.0 0.0 all-gather.14.cloned.1.call-start
  195.1 2.7 fusion.37
  197.8 0.0 all-gather.14.cloned.1.call-update
  197.8 0.7 fusion.35
  198.5 0.7 fusion.34
  199.1 70.7 %all-gather.12.cloned.1.call-done = bf16[2048,1024]{1,0:T(8,128)(2,1)} async-done(((bf16[128,1024]{1,0:T(8,128)(2,1)}), bf16[2048,1024]{1,0:T(8,128)(2,1)}) %all-gather.12.cloned.1.call-update) | async-done | bytes 4194320 | tf_op jit(solution)/shard_map/all_gather | solution.py:96
  269.8 90.5 %all-gather.14.cloned.1.call-done = bf16[1024,2048]{1,0:T(8,128)(2,1)} async-done(((bf16[1024,128]{1,0:T(8,128)(2,1)}), bf16[1024,2048]{1,0:T(8,128)(2,1)}) %all-gather.14.cloned.1.call-update) | async-done | bytes 4194320 | tf_op jit(solution)/shard_map/all_gather | solution.py:97
  360.3 4.8 %copy.58 = bf16[2048,1024]{1,0:T(8,128)(2,1)} copy(bf16[2048,1024]{1,0:T(8,128)(2,1)} %all-gather.12.cloned.1.call-done) | data formatting | bytes 8388608
  365.1 2.0 copy.59
  (28 shorter events, 0.1 us)
Async XLA Ops:
  7.2 29.0 %copy-start = (bf16[512,1024]{1,0:T(8,128)(2,1)S(1)}, bf16[512,1024]{1,0:T(8,128)(2,1)}, u32[]{:S(2)}) copy-start(bf16[512,1024]{1,0:T(8,128)(2,1)} %param.16) | copy-start | bytes 3145732
  7.2 1.5 copy-start.3
  7.2 15.7 %all-gather.8.cloned.1.call-start = ((), (), s32[]{:S(2)}) async-start(), calls=%async_computation.2 | async-start | bytes 3145728 | tf_op jit(solution)/shard_map/all_gather | solution.py:54
  7.9 28.3 %all-gather.6.cloned.1.call-start = ((), (), s32[]{:S(2)}) async-start(), calls=%async_computation.1 | async-start | bytes 3145728 | tf_op jit(solution)/shard_map/all_gather | solution.py:53
  8.7 123.3 %reduce-scatter.4.cloned.1.call-start = ((), (), s32[]{:S(2)}) async-start(), calls=%async_computation.6 | async-start | bytes 2228224 | tf_op jit(solution)/shard_map/reduce_scatter | solution.py:74
  9.0 1.2 copy-start.2
  10.5 0.7 copy-start.15
  11.4 0.9 copy-start.16
  22.9 1.6 copy-start.5
  24.5 2.8 copy-start.8
  31.4 8.9 %copy-start.7 = (bf16[2048,256]{1,0:T(8,128)(2,1)S(1)}, bf16[2048,256]{1,0:T(8,128)(2,1)}, u32[]{:S(2)}) copy-start(bf16[2048,256]{1,0:T(8,128)(2,1)} %param.22) | copy-start | bytes 3145732
  49.1 82.9 %copy-start.11 = (f32[16,1024]{1,0:T(8,128)S(1)}, f32[16,1024]{1,0:T(8,128)}, u32[]{:S(2)}) copy-start(f32[16,1024]{1,0:T(8,128)} %param.29) | copy-start | bytes 196612
  49.1 82.9 %copy-start.12 = (f32[16,1024]{1,0:T(8,128)S(1)}, f32[16,1024]{1,0:T(8,128)}, u32[]{:S(2)}) copy-start(f32[16,1024]{1,0:T(8,128)} %param.27) | copy-start | bytes 196612
  49.1 82.9 %copy-start.13 = (f32[16,1024]{1,0:T(8,128)S(1)}, f32[16,1024]{1,0:T(8,128)}, u32[]{:S(2)}) copy-start(f32[16,1024]{1,0:T(8,128)} %param.28) | copy-start | bytes 196612
  49.1 82.9 %copy-start.14 = (f32[16,1024]{1,0:T(8,128)S(1)}, f32[16,1024]{1,0:T(8,128)}, u32[]{:S(2)}) copy-start(f32[16,1024]{1,0:T(8,128)} %param.26) | copy-start | bytes 196612
  49.2 143.0 %copy-start.9 = (f32[128,1024]{1,0:T(8,128)S(1)}, f32[128,1024]{1,0:T(8,128)}, u32[]{:S(2)}) copy-start(f32[128,1024]{1,0:T(8,128)} %param.24) | copy-start | bytes 1572868
  49.2 145.9 %copy-start.10 = (f32[1024,128]{1,0:T(8,128)S(1)}, f32[1024,128]{1,0:T(8,128)}, u32[]{:S(2)}) copy-start(f32[1024,128]{1,0:T(8,128)} %param.25) | copy-start | bytes 1572868
  49.2 143.0 %all-gather.10.cloned.1.call-start = ((), (), s32[]{:S(2)}) async-start(), calls=%async_computation.3 | async-start | bytes 2228224 | tf_op jit(solution)/shard_map/all_gather | solution.py:80
  133.7 136.1 %all-gather.12.cloned.1.call-start = ((), (), s32[]{:S(2)}) async-start(), calls=%async_computation.4 | async-start | bytes 4456448 | tf_op jit(solution)/shard_map/all_gather | solution.py:96
  192.2 2.9 copy-start.6
  195.0 165.3 %all-gather.14.cloned.1.call-start = ((), (), s32[]{:S(2)}) async-start(), calls=%async_computation.5 | async-start | bytes 4456448 | tf_op jit(solution)/shard_map/all_gather | solution.py:97
  360.3 4.8 %copy-start.4 = (bf16[1024,2048]{1,0:T(8,128)(2,1)S(1)}, bf16[1024,2048]{1,0:T(8,128)(2,1)}, u32[]{:S(2)}) copy-start(bf16[1024,2048]{1,0:T(8,128)(2,1)} %all-gather.14.cloned.1.call-done) | copy-start | bytes 12582916
  365.1 2.0 copy-start.1
Sparse Core Ops, SparseCore 0:
  9.5 13.2 all-gather.7
  24.4 11.7 all-gather.5
  49.3 82.6 reduce-scatter.3
  135.2 56.9 all-gather.9
  195.4 74.3 all-gather.11
  272.9 87.3 all-gather.13
where the time goes:
time: 374 us
  waiting for transfers between devices  319 us (85%)
  matrix products  23.3 us (6%)
  between operations  14.3 us (4%)
  local copies, waits for them, and re-layouts  13.8 us (4%)
    all_gather x1, waiting for transfers between devices, local(): lax.all_gather(output_master.astype(jnp.bfloat16), 'fs', axis=1, tiled=True)  90.5 us
    reduce_scatter x1, waiting for transfers between devices, local(): lax.psum_scatter(partial_value, 'fs', scatter_dimension=0, tiled=True)  82.7 us
    all_gather x1, waiting for transfers between devices, local(): lax.all_gather(value_master.astype(jnp.bfloat16), 'fs', axis=0, tiled=True)  70.7 us
    all_gather x1, waiting for transfers between devices, local(): full_direction = lax.all_gather(direction, 'fs', axis=0, tiled=True)  58.5 us
    unnamed x39, local copies, waits for them, and re-layouts  11.6 us
    dot_general x2, matrix products, contract_rows(): lax.dot_general(left, right, (((0,), (0,)), ((), ())), precision=lax.Prec...  10.9 us
    all_gather x1, waiting for transfers between devices, local(): lax.all_gather(output_cotangent, 'tp', axis=1, tiled=True)  10.5 us
  transfers between devices with their start and end apart: 6, of which 6 were waited for; matrix products, arithmetic and copies ran while one was open for 4% of the time, Pallas kernels for 0%

commit v1 on v0

--- a/solution.py
+++ b/solution.py
@@ -77,7 +77,10 @@
     moment_new = 0.8 * moments + 0.2 * own_rows
     second_new = 0.95 * seconds + 0.05 * own_rows * own_rows
     direction = moment_new / (jnp.sqrt(second_new) + 1e-08)
-    full_direction = lax.all_gather(direction, "fs", axis=0, tiled=True)
+    peers = lax.axis_size("fs")
+    blocks = jnp.stack([direction for _ in range(peers)])
+    blocks = lax.all_to_all(blocks, "fs", split_axis=0, concat_axis=0)
+    full_direction = jnp.concatenate(blocks, axis=0)
     step_value = jnp.dot(
         value_rows,
         full_direction[:, :head_cols],

time: 374 us -> 358 us (0.957)
  waiting for transfers between devices: 319 us -> 298 us
  starting transfers between devices: 0.24 us -> 4.05 us
    all_gather x1 -> x0, waiting for transfers between devices: 58.5 us -> none  [local(): full_direction = lax.all_gather(direction, 'fs', axis=0, tiled=True)]
    all_to_all x0 -> x1, waiting for transfers between devices: none -> 35.2 us  [local(): blocks = lax.all_to_all(blocks, 'fs', split_axis=0, concat_axis=0)]
    all_to_all x0 -> x1, starting transfers between devices: none -> 3.85 us  [local(): blocks = lax.all_to_all(blocks, 'fs', split_axis=0, concat_axis=0)]
    unnamed x39 -> x37, local copies, waits for them, and re-layouts: 11.6 us -> 11.6 us
where the time goes in v1:
time: 358 us; the launch traced here: 357 us
  waiting for transfers between devices  298 us (83%)
  matrix products  22.8 us (6%)
  local copies, waits for them, and re-layouts  15.3 us (4%)
  between operations  14 us (4%)
  starting transfers between devices  4.05 us (1%)
    all_gather x1, waiting for transfers between devices, local(): lax.all_gather(output_master.astype(jnp.bfloat16), 'fs', axis=1, tiled=True)  90.5 us
    reduce_scatter x1, waiting for transfers between devices, local(): lax.psum_scatter(partial_value, 'fs', scatter_dimension=0, tiled=True)  82.9 us
    all_gather x1, waiting for transfers between devices, local(): lax.all_gather(value_master.astype(jnp.bfloat16), 'fs', axis=0, tiled=True)  73.1 us
    all_to_all x1, waiting for transfers between devices, local(): blocks = lax.all_to_all(blocks, 'fs', split_axis=0, concat_axis=0)  35.2 us
    unnamed x37, local copies, waits for them, and re-layouts  11.6 us
    dot_general x2, matrix products, contract_rows(): lax.dot_general(left, right, (((0,), (0,)), ((), ())), precision=lax.Prec...  10.9 us
    all_gather x1, waiting for transfers between devices, local(): lax.all_gather(output_cotangent, 'tp', axis=1, tiled=True)  10.5 us
  transfers between devices with their start and end apart: 6, of which 6 were waited for; matrix products, arithmetic and copies ran while one was open for 4% of the time, Pallas kernels for 0%

profile of v1, /device:TPU:0, one launch (start us, length us, event | category | flops | bytes accessed | tf_op | source)
XLA Modules:
  0.0 357.1 jit_solution(2699826985882291915)
XLA Ops:
  7.2 0.0 copy-start
  7.2 0.0 all-gather.7.cloned.1.call-start
  7.2 0.7 all-gather.7.cloned.1.call-update
  7.9 0.0 all-gather.5.cloned.1.call-start
  8.0 0.7 all-gather.5.cloned.1.call-update
  8.7 0.0 reduce-scatter.4.cloned.1.call-start
  8.7 0.2 convert_bitcast_fusion
  9.0 0.0 copy-start.2
  9.0 0.5 copy.53
  9.5 0.7 copy-done.2
  10.2 0.2 convert_bitcast_fusion.1
  10.5 0.0 copy-start.14
  10.5 0.5 copy.52
  11.0 0.2 copy-done.14
  11.1 0.3 fusion.9
  11.4 0.0 copy-start.15
  11.4 0.6 multiply_reduce_fusion
  12.0 0.1 copy.45
  12.2 0.1 copy.46
  12.3 0.1 broadcast_bitcast_fusion
  12.4 10.5 %all-gather.7.cloned.1.call-done = bf16[512,2048]{1,0:T(8,128)(2,1)} async-done(((bf16[512,1024]{1,0:T(8,128)(2,1)}), bf16[512,2048]{1,0:T(8,128)(2,1)}) %all-gather.7.cloned.1.call-update) | async-done | bytes 2097168 | tf_op jit(solution)/shard_map/all_gather | solution.py:54
  22.9 0.6 mul.105
  23.5 1.0 copy-done.5
  24.5 2.8 fusion.18
  27.3 4.0 %fusion.13 = f32[256,1024]{0,1:T(8,128)S(1)} fusion(bf16[2048,256]{1,0:T(8,128)(2,1)S(1)} %copy-done.7, f32[1024,2048]{1,0:T(8,128)S(1)} %fusion.18), kind=kOutput, calls=%fused_computation.18 | convolution fusion | flops 6444548096 | bytes 10485760 | tf_op jit(solution)/shard_map/dot_general | solution.py:10
  31.4 4.8 %all-gather.5.cloned.1.call-done = bf16[512,2048]{1,0:T(8,128)(2,1)} async-done(((bf16[512,1024]{1,0:T(8,128)(2,1)}), bf16[512,2048]{1,0:T(8,128)(2,1)}) %all-gather.5.cloned.1.call-update) | async-done | bytes 2097168 | tf_op jit(solution)/shard_map/all_gather | solution.py:53
  36.2 4.0 %fusion.38 = f32[2048,1024]{1,0:T(8,128)S(1)} fusion(bf16[512,2048]{1,0:T(8,128)(2,1)} %all-gather.5.cloned.1.call-done, bf16[512,1024]{1,0:T(8,128)(2,1)S(1)} %copy-done), kind=kOutput, calls=%fused_computation.47 | convolution fusion | flops 2147483648 | bytes 11534336 | tf_op jit(solution)/shard_map/dot_general | solution.py:17
  40.2 6.9 %fusion.10 = f32[256,1024]{0,1:T(8,128)S(1)} fusion(bf16[2048,256]{1,0:T(8,128)(2,1)S(1)} %copy-done.6, f32[2048,1024]{1,0:T(8,128)S(1)} %fusion.38), kind=kOutput, calls=%fused_computation.17 | convolution fusion | flops 6444548096 | bytes 10485760 | tf_op jit(solution)/shard_map/dot_general | solution.py:10
  47.2 0.1 pad_maximum_fusion
  47.3 1.8 copy.50
  49.2 0.0 reduce-scatter.4.cloned.1.call-update
  49.2 82.9 %reduce-scatter.4.cloned.1.call-done = f32[16,2048]{1,0:T(8,128)} async-done(((f32[256,2048]{1,0:T(8,128)}), f32[16,2048]{1,0:T(8,128)}) %reduce-scatter.4.cloned.1.call-update) | async-done | bytes 131088 | tf_op jit(solution)/shard_map/reduce_scatter | solution.py:74
  132.1 1.0 add_divide_fusion
  133.1 1.6 stack.2
  134.7 3.9 %all-to-all-start = ((f32[16,16,2048]{2,1,0:T(8,128)}), f32[16,16,2048]{2,1,0:T(8,128)S(1)}, u32[]{:S(2)}, u32[]{:S(2)}) async-start(f32[16,16,2048]{2,1,0:T(8,128)} %stack.2), calls=%async_computation | async-start | bytes 4194304 | tf_op jit(solution)/shard_map/all_to_all | solution.py:82
  138.6 0.0 all-gather.9.cloned.1.call-start
  138.6 35.2 %all-to-all-done = f32[16,16,2048]{2,1,0:T(8,128)S(1)} async-done(((f32[16,16,2048]{2,1,0:T(8,128)}), f32[16,16,2048]{2,1,0:T(8,128)S(1)}, u32[]{:S(2)}, u32[]{:S(2)}) %all-to-all-start) | async-done | bytes 2097184 | tf_op jit(solution)/shard_map/all_to_all | solution.py:82
  173.8 2.2 fusion.36
  176.0 0.0 all-gather.9.cloned.1.call-update
  176.0 0.0 all-gather.11.cloned.1.call-start
  176.1 2.7 fusion.37
  178.8 0.0 all-gather.11.cloned.1.call-update
  178.9 0.7 fusion.35
  179.5 0.7 fusion.34
  180.2 73.1 %all-gather.9.cloned.1.call-done = bf16[2048,1024]{1,0:T(8,128)(2,1)} async-done(((bf16[128,1024]{1,0:T(8,128)(2,1)}), bf16[2048,1024]{1,0:T(8,128)(2,1)}) %all-gather.9.cloned.1.call-update) | async-done | bytes 4194320 | tf_op jit(solution)/shard_map/all_gather | solution.py:99
  253.3 90.5 %all-gather.11.cloned.1.call-done = bf16[1024,2048]{1,0:T(8,128)(2,1)} async-done(((bf16[1024,128]{1,0:T(8,128)(2,1)}), bf16[1024,2048]{1,0:T(8,128)(2,1)}) %all-gather.11.cloned.1.call-update) | async-done | bytes 4194320 | tf_op jit(solution)/shard_map/all_gather | solution.py:100
  343.7 4.8 %copy.59 = bf16[2048,1024]{1,0:T(8,128)(2,1)} copy(bf16[2048,1024]{1,0:T(8,128)(2,1)} %all-gather.9.cloned.1.call-done) | data formatting | bytes 8388608
  348.6 2.0 copy.60
  (26 shorter events, 0.1 us)
Async XLA Ops:
  7.2 29.0 %copy-start = (bf16[512,1024]{1,0:T(8,128)(2,1)S(1)}, bf16[512,1024]{1,0:T(8,128)(2,1)}, u32[]{:S(2)}) copy-start(bf16[512,1024]{1,0:T(8,128)(2,1)} %param.16) | copy-start | bytes 3145732
  7.2 1.5 copy-start.3
  7.2 15.7 %all-gather.7.cloned.1.call-start = ((), (), s32[]{:S(2)}) async-start(), calls=%async_computation.3 | async-start | bytes 3145728 | tf_op jit(solution)/shard_map/all_gather | solution.py:54
  7.9 28.3 %all-gather.5.cloned.1.call-start = ((), (), s32[]{:S(2)}) async-start(), calls=%async_computation.2 | async-start | bytes 3145728 | tf_op jit(solution)/shard_map/all_gather | solution.py:53
  8.7 123.4 %reduce-scatter.4.cloned.1.call-start = ((), (), s32[]{:S(2)}) async-start(), calls=%async_computation.6 | async-start | bytes 2228224 | tf_op jit(solution)/shard_map/reduce_scatter | solution.py:74
  9.0 1.2 copy-start.2
  10.5 0.7 copy-start.14
  11.4 0.9 copy-start.15
  22.9 1.6 copy-start.5
  24.5 2.8 copy-start.7
  31.4 8.9 %copy-start.6 = (bf16[2048,256]{1,0:T(8,128)(2,1)S(1)}, bf16[2048,256]{1,0:T(8,128)(2,1)}, u32[]{:S(2)}) copy-start(bf16[2048,256]{1,0:T(8,128)(2,1)} %param.22) | copy-start | bytes 3145732
  49.1 83.0 %copy-start.10 = (f32[16,1024]{1,0:T(8,128)S(1)}, f32[16,1024]{1,0:T(8,128)}, u32[]{:S(2)}) copy-start(f32[16,1024]{1,0:T(8,128)} %param.29) | copy-start | bytes 196612
  49.1 83.0 %copy-start.11 = (f32[16,1024]{1,0:T(8,128)S(1)}, f32[16,1024]{1,0:T(8,128)}, u32[]{:S(2)}) copy-start(f32[16,1024]{1,0:T(8,128)} %param.27) | copy-start | bytes 196612
  49.1 83.0 %copy-start.12 = (f32[16,1024]{1,0:T(8,128)S(1)}, f32[16,1024]{1,0:T(8,128)}, u32[]{:S(2)}) copy-start(f32[16,1024]{1,0:T(8,128)} %param.28) | copy-start | bytes 196612
  49.1 83.0 %copy-start.13 = (f32[16,1024]{1,0:T(8,128)S(1)}, f32[16,1024]{1,0:T(8,128)}, u32[]{:S(2)}) copy-start(f32[16,1024]{1,0:T(8,128)} %param.26) | copy-start | bytes 196612
  134.7 39.1 %copy-start.8 = (f32[128,1024]{1,0:T(8,128)S(1)}, f32[128,1024]{1,0:T(8,128)}, u32[]{:S(2)}) copy-start(f32[128,1024]{1,0:T(8,128)} %param.24) | copy-start | bytes 1572868
  134.7 39.1 %all-to-all-start = ((f32[16,16,2048]{2,1,0:T(8,128)}), f32[16,16,2048]{2,1,0:T(8,128)S(1)}, u32[]{:S(2)}, u32[]{:S(2)}) async-start(f32[16,16,2048]{2,1,0:T(8,128)} %stack.2), calls=%async_computation | async-start | bytes 4194304 | tf_op jit(solution)/shard_map/all_to_all | solution.py:82
  138.5 37.5 %copy-start.9 = (f32[1024,128]{1,0:T(8,128)S(1)}, f32[1024,128]{1,0:T(8,128)}, u32[]{:S(2)}) copy-start(f32[1024,128]{1,0:T(8,128)} %param.25) | copy-start | bytes 1572868
  138.6 114.7 %all-gather.9.cloned.1.call-start = ((), (), s32[]{:S(2)}) async-start(), calls=%async_computation.4 | async-start | bytes 4456448 | tf_op jit(solution)/shard_map/all_gather | solution.py:99
  176.0 167.7 %all-gather.11.cloned.1.call-start = ((), (), s32[]{:S(2)}) async-start(), calls=%async_computation.5 | async-start | bytes 4456448 | tf_op jit(solution)/shard_map/all_gather | solution.py:100
  343.7 4.8 %copy-start.4 = (bf16[1024,2048]{1,0:T(8,128)(2,1)S(1)}, bf16[1024,2048]{1,0:T(8,128)(2,1)}, u32[]{:S(2)}) copy-start(bf16[1024,2048]{1,0:T(8,128)(2,1)} %all-gather.11.cloned.1.call-done) | copy-start | bytes 12582916
  348.6 2.0 copy-start.1
Sparse Core Ops, SparseCore 0:
  9.5 13.2 all-gather.6
  24.4 11.7 all-gather.4
  49.3 82.7 reduce-scatter.3
  176.2 77.0 all-gather.8
  256.4 87.3 all-gather.10
